TPU v7x, 32 devices: a whole 2x2x4 slice. The times are simulated.
32 devices in a mesh: fs: 16 (over z, y, x), tp: 2 (over core).
Axes of the slice: x: 2, y: 2, z: 4, core: 2. Of those that a mesh axis runs over, the one named last changes fastest.
Arguments:
- tokens: bfloat16 [12288, 2048], P('fs'), may hold values from -6 to 6
- norm_gain: float32 [2048], replicated, may hold values from 0.1 to 1.9
- up_weight: float32 [2048, 8192], P('fs', 'tp'), may hold values from -0.125 to 0.125
- up_scale: float32 [8192], P('tp'), may hold values from 0.5 to 2
- down_weight: float32 [8192, 2048], P('tp', 'fs'), may hold values from -0.09375 to 0.09375
- down_scale: float32 [1, 2048], replicated, may hold values from 0.5 to 2
Outputs:
- mixed: bfloat16 [12288, 2048], P('fs', 'tp')
All inputs are finite; a program needn't handle non-finite values.
Results may differ from a plain program's by a relative error of at most 0.014.
Values may be sent and summed in bfloat16 or wider, within the bound.
A program may use at most 128 MiB of HBM per device.

v0:
```python
import jax
import jax.numpy as jnp
from jax import lax
from jax.sharding import PartitionSpec as P


def on_device(tokens, norm_gain, up_weight, up_scale, down_weight, down_scale):
    values = tokens.astype(jnp.float32)
    normed = (
        values * lax.rsqrt(jnp.mean(values * values, axis=-1, keepdims=True) + 1e-06) * norm_gain
    ).astype(jnp.bfloat16)
    up_cast = up_weight.astype(jnp.bfloat16)
    down_cast = down_weight.astype(jnp.bfloat16)
    up_full = lax.all_gather(up_cast, "fs", axis=0, tiled=True)
    pre = jnp.dot(normed, up_full, preferred_element_type=jnp.float32) * up_scale
    hidden = jnp.square(jnp.maximum(pre, 0.0)).astype(jnp.bfloat16)
    down_full = lax.all_gather(down_cast, "fs", axis=1, tiled=True)
    partial_value = jnp.dot(hidden, down_full, preferred_element_type=jnp.float32) * down_scale
    rounded = partial_value.astype(jnp.bfloat16)
    return (
        lax.psum_scatter(rounded, "tp", scatter_dimension=1, tiled=True)
        .astype(jnp.float32)
        .astype(jnp.bfloat16)
    )


def solution(mesh):
    in_specs = (P("fs", None), P(), P("fs", "tp"), P("tp"), P("tp", "fs"), P())
    out_specs = P("fs", "tp")
    return jax.shard_map(
        on_device, mesh=mesh, in_specs=in_specs, out_specs=out_specs, check_vma=False
    )
```

profile of v0, /device:TPU:0, one launch (start us, length us, event | category | flops | bytes accessed | tf_op | source)
XLA Modules:
  0.0 508.0 jit_solution(3920290398394496879)
XLA Ops:
  6.5 0.0 copy-start
  6.5 0.0 copy-start.2
  6.5 0.0 copy-start.1
  6.5 0.0 copy-start.3
  6.5 0.0 all-gather.3.cloned.1.call-start
  6.6 2.8 convert_element_type.22
  9.4 0.0 all-gather.3.cloned.1.call-update
  9.5 0.0 all-gather.5.cloned.1.call-start
  9.5 2.7 convert_element_type.24
  12.2 0.0 all-gather.5.cloned.1.call-update
  12.2 0.0 reduce-scatter.2.cloned.1.call-start
  12.2 0.0 copy-done
  12.3 0.7 fusion
  13.0 190.9 %all-gather.3.cloned.1.call-done = bf16[2048,4096]{1,0:T(8,128)(2,1)} async-done(((bf16[128,4096]{1,0:T(8,128)(2,1)}), bf16[2048,4096]{1,0:T(8,128)(2,1)}) %all-gather.3.cloned.1.call-update) | async-done | bytes 16777232 | tf_op jit(solution)/shard_map/all_gather | solution.py:14
  203.9 250.0 %all-gather.5.cloned.1.call-done = bf16[4096,2048]{1,0:T(8,128)(2,1)} async-done(((bf16[4096,128]{1,0:T(8,128)(2,1)}), bf16[4096,2048]{1,0:T(8,128)(2,1)}) %all-gather.5.cloned.1.call-update) | async-done | bytes 16777232 | tf_op jit(solution)/shard_map/all_gather | solution.py:17
  453.9 0.0 copy-done.2
  453.9 0.0 copy-done.1
  453.9 0.0 copy-done.3
  453.9 38.3 %multiply_convert_fusion.1 = bf16[768,2048]{1,0:T(8,128)(2,1)} fusion(bf16[4096,2048]{1,0:T(8,128)(2,1)} %all-gather.5.cloned.1.call-done, f32[2048]{0:T(1024)S(1)} %bitcast.8, bf16[2048,4096]{1,0:T(8,128)(2,1)} %all-gather.3.cloned.1.call-done, f32[4096]{0:T(1024)S(1)} %copy-done.1, bf16[768,2048]{1,0:T(8,128)(2,1)S(1)} %copy-done, f32[2048]{0:T(1024)S(1)} %copy-done.3, ...), kind=kOutput, calls=%fused_computation.6 | convolution fusion | flops 25791823872 | bytes 39881728 | tf_op jit(solution)/shard_map/dot_general | solution.py:18
  492.2 0.0 reduce-scatter.2.cloned.1.call-update
  492.2 9.3 %reduce-scatter.2.cloned.1.call-done = bf16[768,1024]{1,0:T(8,128)(2,1)} async-done(((bf16[768,2048]{1,0:T(8,128)(2,1)}), bf16[768,1024]{1,0:T(8,128)(2,1)}) %reduce-scatter.2.cloned.1.call-update) | async-done | bytes 1572880 | tf_op jit(solution)/shard_map/reduce_scatter | solution.py:21
  (1 shorter events, 0.0 us)
Async XLA Ops:
  6.5 5.7 %copy-start = (bf16[768,2048]{1,0:T(8,128)(2,1)S(1)}, bf16[768,2048]{1,0:T(8,128)(2,1)}, u32[]{:S(2)}) copy-start(bf16[768,2048]{1,0:T(8,128)(2,1)} %param.6) | copy-start | bytes 9437188
  6.5 447.4 %copy-start.2 = (f32[1,2048]{1,0:T(1,128)S(1)}, f32[1,2048]{1,0:T(1,128)}, u32[]{:S(2)}) copy-start(f32[1,2048]{1,0:T(1,128)} %param.11) | copy-start | bytes 24580
  6.5 447.4 %copy-start.1 = (f32[4096]{0:T(1024)S(1)}, f32[4096]{0:T(1024)}, u32[]{:S(2)}) copy-start(f32[4096]{0:T(1024)} %param.9) | copy-start | bytes 49156
  6.5 447.4 %copy-start.3 = (f32[2048]{0:T(1024)S(1)}, f32[2048]{0:T(1024)}, u32[]{:S(2)}) copy-start(f32[2048]{0:T(1024)} %param.7) | copy-start | bytes 24580
  6.5 197.3 %all-gather.3.cloned.1.call-start = ((), (), s32[]{:S(2)}) async-start(), calls=%async_computation.1 | async-start | bytes 17825792 | tf_op jit(solution)/shard_map/all_gather | solution.py:14
  9.5 444.4 %all-gather.5.cloned.1.call-start = ((), (), s32[]{:S(2)}) async-start(), calls=%async_computation.2 | async-start | bytes 17825792 | tf_op jit(solution)/shard_map/all_gather | solution.py:17
  12.2 489.3 %reduce-scatter.2.cloned.1.call-start = ((), (), s32[]{:S(2)}) async-start(), calls=%async_computation.3 | async-start | bytes 4718592 | tf_op jit(solution)/shard_map/reduce_scatter | solution.py:21
Sparse Core Ops, SparseCore 0:
  10.1 193.7 all-gather.2
  206.6 247.2 all-gather.4
  492.3 9.1 reduce-scatter.1
where the time goes:
time: 508 us
  waiting for transfers between devices  450 us (89%)
  matrix products  38.3 us (8%)
  between operations  13.1 us (3%)
  other arithmetic  6.2 us (1%)
    all_gather x1, waiting for transfers between devices, on_device(): down_full = lax.all_gather(down_cast, 'fs', axis=1, tiled=True)  250 us
    all_gather x1, waiting for transfers between devices, on_device(): up_full = lax.all_gather(up_cast, 'fs', axis=0, tiled=True)  191 us
    dot_general x1, matrix products, on_device(): jnp.dot(hidden, down_full, preferred_element_type=jnp.float32) * down_scale  38.3 us
  transfers between devices with their start and end apart: 3, of which 3 were waited for; matrix products, arithmetic and copies ran while one was open for 1% of the time, Pallas kernels for 0%

commit v1 on v0

--- a/solution.py
+++ b/solution.py
@@ -14,7 +14,7 @@
     up_full = lax.all_gather(up_cast, "fs", axis=0, tiled=True)
     pre = jnp.dot(normed, up_full, preferred_element_type=jnp.float32) * up_scale
     hidden = jnp.square(jnp.maximum(pre, 0.0)).astype(jnp.bfloat16)
-    down_full = lax.all_gather(down_cast, "fs", axis=1, tiled=True)
+    down_full = jnp.concatenate(lax.all_gather(down_cast, "fs"), axis=1)
     partial_value = jnp.dot(hidden, down_full, preferred_element_type=jnp.float32) * down_scale
     rounded = partial_value.astype(jnp.bfloat16)
     return (

time: 508 us -> 451 us (0.89)
  waiting for transfers between devices: 450 us -> 371 us
  local copies, waits for them, and re-layouts: 0.01 us -> 21 us
    all_gather x1, waiting for transfers between devices: 250 us -> 191 us  [on_device(): down_full = jnp.concatenate(lax.all_gather(down_cast, 'fs'), axis=1)]
    reshape x0 -> x1, local copies, waits for them, and re-layouts: none -> 21 us  [on_device(): down_full = jnp.concatenate(lax.all_gather(down_cast, 'fs'), axis=1)]
    all_gather x1, waiting for transfers between devices: 191 us -> 171 us  [on_device(): up_full = lax.all_gather(up_cast, 'fs', axis=0, tiled=True)]
    dot_general x1, matrix products: 38.3 us -> 19.8 us  [on_device(): jnp.dot(hidden, down_full, preferred_element_type=jnp.float32) * down_scale]
    dot_general x0 -> x1, matrix products: none -> 18.5 us  [on_device(): jnp.dot(normed, up_full, preferred_element_type=jnp.float32) * up_scale]
  transfers between devices with their start and end apart: 3 -> 3, of which waited for: 3 -> 3; matrix products, arithmetic and copies ran while one was open for 1% -> 5% of each run, Pallas kernels for 0% -> 0%
where the time goes in v1:
time: 451 us; the launch traced here: 450 us
  waiting for transfers between devices  371 us (82%)
  matrix products  38.2 us (8%)
  local copies, waits for them, and re-layouts  21 us (5%)
  between operations  13.1 us (3%)
  other arithmetic  6.2 us (1%)
    all_gather x1, waiting for transfers between devices, on_device(): down_full = jnp.concatenate(lax.all_gather(down_cast, 'fs'), axis=1)  191 us
    all_gather x1, waiting for transfers between devices, on_device(): up_full = lax.all_gather(up_cast, 'fs', axis=0, tiled=True)  171 us
    reshape x1, local copies, waits for them, and re-layouts, on_device(): down_full = jnp.concatenate(lax.all_gather(down_cast, 'fs'), axis=1)  21 us
    dot_general x1, matrix products, on_device(): jnp.dot(hidden, down_full, preferred_element_type=jnp.float32) * down_scale  19.8 us
    dot_general x1, matrix products, on_device(): jnp.dot(normed, up_full, preferred_element_type=jnp.float32) * up_scale  18.5 us
    reduce_scatter x1, waiting for transfers between devices, on_device(): lax.psum_scatter(rounded, 'tp', scatter_dimension=1, tiled=True)  9.32 us
  transfers between devices with their start and end apart: 3, of which 3 were waited for; matrix products, arithmetic and copies ran while one was open for 5% of the time, Pallas kernels for 0%

profile of v1, /device:TPU:0, one launch (start us, length us, event | category | flops | bytes accessed | tf_op | source)
XLA Modules:
  0.0 449.9 jit_solution(5662449550664147701)
XLA Ops:
  6.5 0.0 copy-start
  6.5 0.0 all-gather.6.cloned.1.call-start
  6.5 2.8 convert_element_type.24
  9.4 0.0 all-gather.6.cloned.1.call-update
  9.4 0.0 all-gather.4.cloned.1.call-start
  9.4 2.7 convert_element_type.22
  12.1 0.0 all-gather.4.cloned.1.call-update
  12.1 0.0 reduce-scatter.2.cloned.1.call-start
  12.2 0.0 copy-done
  12.2 0.7 fusion
  12.9 191.0 %all-gather.6.cloned.1.call-done = bf16[65536,128]{1,0:T(8,128)(2,1)} async-done(((bf16[4096,128]{1,0:T(8,128)(2,1)}), bf16[65536,128]{1,0:T(8,128)(2,1)}) %all-gather.6.cloned.1.call-update) | async-done | bytes 16777232 | tf_op jit(solution)/shard_map/all_gather | solution.py:17
  203.9 0.0 copy-start.1
  203.9 0.0 copy-start.2
  203.9 21.0 %copy.7 = bf16[4096,16,128]{0,2,1:T(8,128)(2,1)} copy(bf16[4096,16,128]{2,0,1:T(8,128)(2,1)} %bitcast.20) | data formatting | bytes 33554432 | tf_op jit(solution)/shard_map/reshape | solution.py:17
  224.9 0.0 copy-start.3
  224.9 171.0 %all-gather.4.cloned.1.call-done = bf16[2048,4096]{1,0:T(8,128)(2,1)} async-done(((bf16[128,4096]{1,0:T(8,128)(2,1)}), bf16[2048,4096]{1,0:T(8,128)(2,1)}) %all-gather.4.cloned.1.call-update) | async-done | bytes 16777232 | tf_op jit(solution)/shard_map/all_gather | solution.py:14
  395.8 0.0 copy-done.1
  395.8 0.0 copy-done.2
  395.8 18.5 %fusion.26 = bf16[768,4096]{1,0:T(8,128)(2,1)} fusion(f32[4096]{0:T(1024)S(1)} %copy-done.1, bf16[2048,4096]{1,0:T(8,128)(2,1)} %all-gather.4.cloned.1.call-done, bf16[768,2048]{1,0:T(8,128)(2,1)S(1)} %copy-done, f32[2048]{0:T(1024)S(1)} %copy-done.2, f32[768]{0:T(1024)S(1)} %add_rsqrt_fusion), kind=kOutput, calls=%bitcast_fusion.clone.1 | convolution fusion | flops 12903776256 | bytes 26242048 | tf_op jit(solution)/shard_map/dot_general | solution.py:15
  414.3 0.0 copy-done.3
  414.3 19.8 %multiply_convert_fusion.1 = bf16[768,2048]{1,0:T(8,128)(2,1)} fusion(bf16[4096,2048]{0,1:T(8,128)(2,1)} %bitcast.21, f32[2048]{0:T(1024)S(1)} %bitcast.22, bf16[768,4096]{1,0:T(8,128)(2,1)} %fusion.26), kind=kOutput, calls=%fused_computation.6 | convolution fusion | flops 12888047616 | bytes 26222592 | tf_op jit(solution)/shard_map/dot_general | solution.py:18
  434.1 0.0 reduce-scatter.2.cloned.1.call-update
  434.1 9.3 %reduce-scatter.2.cloned.1.call-done = bf16[768,1024]{1,0:T(8,128)(2,1)} async-done(((bf16[768,2048]{1,0:T(8,128)(2,1)}), bf16[768,1024]{1,0:T(8,128)(2,1)}) %reduce-scatter.2.cloned.1.call-update) | async-done | bytes 1572880 | tf_op jit(solution)/shard_map/reduce_scatter | solution.py:21
  (1 shorter events, 0.0 us)
Async XLA Ops:
  6.5 5.7 %copy-start = (bf16[768,2048]{1,0:T(8,128)(2,1)S(1)}, bf16[768,2048]{1,0:T(8,128)(2,1)}, u32[]{:S(2)}) copy-start(bf16[768,2048]{1,0:T(8,128)(2,1)} %param.6) | copy-start | bytes 9437188
  6.5 197.3 %all-gather.6.cloned.1.call-start = ((), (), s32[]{:S(2)}) async-start(), calls=%async_computation.3 | async-start | bytes 17825792 | tf_op jit(solution)/shard_map/all_gather | solution.py:17
  9.4 386.5 %all-gather.4.cloned.1.call-start = ((), (), s32[]{:S(2)}) async-start(), calls=%async_computation.1 | async-start | bytes 17825792 | tf_op jit(solution)/shard_map/all_gather | solution.py:14
  12.1 431.3 %reduce-scatter.2.cloned.1.call-start = ((), (), s32[]{:S(2)}) async-start(), calls=%async_computation.2 | async-start | bytes 4718592 | tf_op jit(solution)/shard_map/reduce_scatter | solution.py:21
  203.9 192.0 %copy-start.1 = (f32[4096]{0:T(1024)S(1)}, f32[4096]{0:T(1024)}, u32[]{:S(2)}) copy-start(f32[4096]{0:T(1024)} %param.9) | copy-start | bytes 49156
  203.9 192.0 %copy-start.2 = (f32[2048]{0:T(1024)S(1)}, f32[2048]{0:T(1024)}, u32[]{:S(2)}) copy-start(f32[2048]{0:T(1024)} %param.7) | copy-start | bytes 24580
  224.9 189.4 %copy-start.3 = (f32[1,2048]{1,0:T(1,128)S(1)}, f32[1,2048]{1,0:T(1,128)}, u32[]{:S(2)}) copy-start(f32[1,2048]{1,0:T(1,128)} %param.11) | copy-start | bytes 24580
Sparse Core Ops, SparseCore 0:
  10.1 193.7 all-gather.5
  206.6 189.1 all-gather.3
  434.2 9.1 reduce-scatter.1
